TPU v7x, 32 devices: a whole 2x2x4 slice. The times are simulated.
32 devices in a mesh: sp: 8 (over z, y), tp: 4 (over x, core).
Axes of the slice: x: 2, y: 2, z: 4, core: 2. Of those that a mesh axis runs over, the one named last changes fastest.
Arguments:
- residual_input_stream: bfloat16 [8192, 2048], P(('sp', 'tp')), may hold values from -6 to 6
- receptance: bfloat16 [8192, 1024], P('sp', 'tp'), may hold values from -6 to 6
- key_matrix_all: bfloat16 [8192, 1024], P('sp', 'tp'), may hold values from -6 to 6
- value_matrix_all: bfloat16 [8192, 1024], P('sp', 'tp'), may hold values from -6 to 6
- decay_preactivation: bfloat16 [8192, 1024], P('sp', 'tp'), may hold values from -15 to 1
- learning_rate_preactivation: bfloat16 [8192, 1024], P('sp', 'tp'), may hold values from -11 to 5
- output_gate_all_heads: bfloat16 [8192, 1024], P('sp', 'tp'), may hold values from -6 to 6
- extra_log_decay: float32 [8192, 1024], P('sp', 'tp'), may hold values from -0.7 to 0
- head_norm_gain: float32 [1024], P('tp'), may hold values from 0.1 to 1.9
- output_projection_weight: bfloat16 [1024, 2048], P('tp'), may hold values from -0.1875 to 0.1875
- feedforward_norm_gain: float32 [2048], replicated, may hold values from 0.1 to 1.9
- gate_projection_weight: bfloat16 [2048, 5632], P('sp', 'tp'), may hold values from -0.125 to 0.125
- up_projection_weight: bfloat16 [2048, 5632], P('sp', 'tp'), may hold values from -0.125 to 0.125
- down_projection_weight: bfloat16 [2048, 5632], P('sp', 'tp'), may hold values from -0.078125 to 0.078125
- convolution_kernel: bfloat16 [3, 2, 5632], P(None, None, 'tp'), may hold values from -3.5 to 3.5
Outputs:
- layer_out: bfloat16 [8192, 2048], P(('sp', 'tp'))
All inputs are finite; a program needn't handle non-finite values.
Results may differ from a plain program's by a relative error of at most 0.022.
Values may be sent and summed in bfloat16 or wider, within the bound.
A program may use at most 128 MiB of HBM per device.

v0:
```python
import jax
import jax.numpy as jnp
from jax import lax
from jax.sharding import PartitionSpec as P

HEAD_WIDTH = 64


highest = lax.Precision.HIGHEST


def entering(x, axis, join, neutral):
    place = lax.axis_index(axis)
    gathered = jax.tree.map(
        lambda a, kind: lax.all_gather(a.astype(kind), axis), x, (jnp.bfloat16, jnp.bfloat16)
    )
    state = jax.tree.map(lambda a, e: jnp.zeros_like(a) + jnp.asarray(e, a.dtype), x, neutral)

    def one(step, state):
        return join(
            state,
            jax.tree.map(
                lambda a, own: lax.dynamic_index_in_dim(a, step, 0, False).astype(own.dtype),
                gathered,
                x,
            ),
        )

    return lax.fori_loop(0, place, one, state)


def passed_along(x, axis, by):
    count = lax.axis_size(axis)
    pairs = [(i, i + by) for i in range(count) if 0 <= i + by < count]
    return lax.ppermute(x, axis, pairs)


def per_head_layout(values_in, number_of_heads):
    return values_in.astype(jnp.float32).reshape(values_in.shape[0], number_of_heads, HEAD_WIDTH)


def block_step(carried, block_in):
    queries, keys, normed_keys, removal, decay_logarithm, values_aug = block_in
    span_len = queries.shape[0]
    cumulative = jnp.cumsum(decay_logarithm, axis=0)
    previous = cumulative - decay_logarithm
    middle = cumulative[span_len // 2]
    scaled_query = queries * jnp.exp(cumulative - middle)
    scaled_normed = normed_keys * jnp.exp(previous - middle)
    scaled_key = keys * jnp.exp(middle - cumulative)
    scaled_removal = removal * jnp.exp(middle - cumulative)
    position = lax.broadcasted_iota(jnp.int32, (span_len, span_len), 0)
    other_pos = lax.broadcasted_iota(jnp.int32, (span_len, span_len), 1)
    strict = (position > other_pos)[None]
    within = (position >= other_pos)[None]
    key_for_rate = jnp.where(
        strict, jnp.einsum("thk,shk->hts", scaled_normed, scaled_key, precision=highest), 0.0
    )
    removal_for_rate = jnp.where(
        strict, jnp.einsum("thk,shk->hts", scaled_normed, scaled_removal, precision=highest), 0.0
    )
    key_for_out = jnp.where(
        within, jnp.einsum("thk,shk->hts", scaled_query, scaled_key, precision=highest), 0.0
    )
    removal_for_out = jnp.where(
        within, jnp.einsum("thk,shk->hts", scaled_query, scaled_removal, precision=highest), 0.0
    )
    right_side = jnp.einsum(
        "thk,hrk->htr", normed_keys * jnp.exp(previous), carried, precision=highest
    )
    right_side = right_side + jnp.einsum(
        "hts,shr->htr", key_for_rate, values_aug, precision=highest
    )
    unit_lower = removal_for_rate + jnp.eye(span_len, dtype=jnp.float32)[None]
    corrections = jax.scipy.linalg.solve_triangular(
        unit_lower, right_side, lower=True, unit_diagonal=True
    )
    readout = jnp.einsum("thk,hrk->thr", queries * jnp.exp(cumulative), carried, precision=highest)
    readout = readout + jnp.einsum("hts,shr->thr", key_for_out, values_aug, precision=highest)
    readout = readout - jnp.einsum("hts,hsr->thr", removal_for_out, corrections, precision=highest)
    to_end = jnp.exp(cumulative[-1][None] - cumulative)
    updated = carried * jnp.exp(cumulative[-1])[:, None, :]
    updated = updated + jnp.einsum("shr,shk->hrk", values_aug, keys * to_end, precision=highest)
    updated = updated - jnp.einsum("hsr,shk->hrk", corrections, removal * to_end, precision=highest)
    return (updated, readout)


def short_convolution_step(
    receptance,
    key_matrix_all,
    value_matrix_all,
    decay_preactivation,
    learning_rate_preactivation,
    extra_log_decay,
):
    number_of_tokens, local_width = receptance.shape
    number_of_heads = local_width // HEAD_WIDTH
    queries = per_head_layout(receptance, number_of_heads)
    keys = per_head_layout(key_matrix_all, number_of_heads)
    values = per_head_layout(value_matrix_all, number_of_heads)
    decay_logarithm = -jnp.exp(
        -jax.nn.softplus(-per_head_layout(decay_preactivation, number_of_heads)) - 0.5
    ) + extra_log_decay.reshape(number_of_tokens, number_of_heads, HEAD_WIDTH)
    rates = jax.nn.sigmoid(per_head_layout(learning_rate_preactivation, number_of_heads))
    normed_keys = keys * lax.rsqrt(jnp.sum(keys * keys, axis=-1, keepdims=True) + 1e-06)
    removal = normed_keys * rates
    values_aug = jnp.concatenate([values, jnp.zeros_like(values)], axis=-1)
    block_count = number_of_tokens // 64

    def blocked(array_in):
        return array_in.reshape(block_count, 64, number_of_heads, array_in.shape[-1])

    start_state = jnp.concatenate(
        [
            jnp.zeros((number_of_heads, HEAD_WIDTH, HEAD_WIDTH), jnp.float32),
            jnp.broadcast_to(
                jnp.eye(HEAD_WIDTH, dtype=jnp.float32), (number_of_heads, HEAD_WIDTH, HEAD_WIDTH)
            ),
        ],
        axis=1,
    )
    final_state, readouts = lax.scan(
        block_step,
        start_state,
        tuple(
            (
                blocked(member)
                for member in (queries, keys, normed_keys, removal, decay_logarithm, values_aug)
            )
        ),
    )
    return (readouts.reshape(number_of_tokens, number_of_heads, 2 * HEAD_WIDTH), final_state)


def compose_maps(first_map, second_map):
    product = jnp.einsum("hij,hjk->hik", first_map[0], second_map[0], precision=highest)
    offset = (
        jnp.einsum("hvj,hjk->hvk", first_map[1], second_map[0], precision=highest) + second_map[1]
    )
    return (product, offset)


def conv_mix(before_rows, current, taps):
    extended = jnp.concatenate([before_rows, current], axis=0).astype(jnp.float32)
    return taps[0] * extended[:-2] + taps[1] * extended[1:-1] + taps[2] * extended[2:]


def body(
    residual_input_stream,
    receptance,
    key_matrix_all,
    value_matrix_all,
    decay_preactivation,
    learning_rate_preactivation,
    output_gate_all_heads,
    extra_log_decay,
    head_norm_gain,
    output_projection_weight,
    feedforward_norm_gain,
    gate_projection_weight,
    up_projection_weight,
    down_projection_weight,
    convolution_kernel,
):
    full_gate, full_up, full_down = (
        lax.all_gather(gate_projection_weight, "sp", axis=0, tiled=True),
        lax.all_gather(up_projection_weight, "sp", axis=0, tiled=True),
        lax.all_gather(down_projection_weight, "sp", axis=0, tiled=True),
    )
    number_of_tokens, local_width = receptance.shape
    number_of_heads = local_width // HEAD_WIDTH
    readouts, final_state = short_convolution_step(
        receptance,
        key_matrix_all,
        value_matrix_all,
        decay_preactivation,
        learning_rate_preactivation,
        extra_log_decay,
    )
    identity_map = (
        jnp.broadcast_to(
            jnp.eye(HEAD_WIDTH, dtype=jnp.float32), (number_of_heads, HEAD_WIDTH, HEAD_WIDTH)
        ),
        jnp.zeros((number_of_heads, HEAD_WIDTH, HEAD_WIDTH), jnp.float32),
    )
    prefix_map = entering(
        (final_state[:, HEAD_WIDTH:], final_state[:, :HEAD_WIDTH]), "sp", compose_maps, identity_map
    )
    readout = readouts[..., :HEAD_WIDTH] + jnp.einsum(
        "thk,hvk->thv", readouts[..., HEAD_WIDTH:], prefix_map[1], precision=highest
    )
    centered = readout - jnp.mean(readout, axis=-1, keepdims=True)
    variance = jnp.mean(centered * centered, axis=-1, keepdims=True)
    normalized = (centered * lax.rsqrt(variance + 0.00064)).reshape(number_of_tokens, local_width)
    mixed_out = (normalized * head_norm_gain * output_gate_all_heads.astype(jnp.float32)).astype(
        jnp.bfloat16
    )
    attention = lax.psum_scatter(
        jnp.dot(mixed_out, output_projection_weight, preferred_element_type=jnp.float32).astype(
            jnp.bfloat16
        ),
        "tp",
        scatter_dimension=0,
        tiled=True,
    ).astype(jnp.float32)
    stream = lax.optimization_barrier(
        (residual_input_stream.astype(jnp.float32) + attention).astype(jnp.bfloat16)
    )
    stream_wide = stream.astype(jnp.float32)
    normed = (
        stream_wide
        * lax.rsqrt(jnp.mean(stream_wide * stream_wide, axis=-1, keepdims=True) + 1e-06)
        * feedforward_norm_gain
    ).astype(jnp.bfloat16)
    whole_rows = lax.all_gather(normed, "tp", axis=0, tiled=True)
    gate_acc = jnp.dot(whole_rows, full_gate, preferred_element_type=jnp.float32)
    up_acc = jnp.dot(whole_rows, full_up, preferred_element_type=jnp.float32)
    gate_pre = gate_acc.astype(jnp.bfloat16)
    up_pre = up_acc.astype(jnp.bfloat16)
    before = passed_along((gate_pre[-2:], up_pre[-2:]), "sp", 1)
    taps = convolution_kernel.astype(jnp.float32)
    gate_mix = conv_mix(before[0], gate_pre, taps[:, 0])
    up_mix = conv_mix(before[1], up_pre, taps[:, 1])
    hidden = (jax.nn.silu(gate_mix) * up_mix).astype(jnp.bfloat16)
    ffn = lax.psum_scatter(
        lax.dot_general(
            hidden, full_down, (((1,), (1,)), ((), ())), preferred_element_type=jnp.float32
        ).astype(jnp.bfloat16),
        "tp",
        scatter_dimension=0,
        tiled=True,
    ).astype(jnp.float32)
    return (stream_wide + ffn).astype(jnp.bfloat16)


def solution(mesh):
    in_specs = (
        P(("sp", "tp"), None),
        P("sp", "tp"),
        P("sp", "tp"),
        P("sp", "tp"),
        P("sp", "tp"),
        P("sp", "tp"),
        P("sp", "tp"),
        P("sp", "tp"),
        P("tp"),
        P("tp", None),
        P(),
        P("sp", "tp"),
        P("sp", "tp"),
        P("sp", "tp"),
        P(None, None, "tp"),
    )
    out_specs = P(("sp", "tp"), None)
    return jax.shard_map(body, mesh=mesh, in_specs=in_specs, out_specs=out_specs, check_vma=False)
```

profile of v0, /device:TPU:0, one launch (start us, length us, event | category | flops | bytes accessed | tf_op | source)
XLA Modules:
  0.0 1008.5 jit_solution(195188094715497504)
XLA Ops:
  49.0 471.9 %while.24 = (s32[]{:T(128)}, f32[4,128,64]{1,2,0:T(8,128)S(1)}, f32[16,64,4,128]{3,1,0,2:T(8,128)}, f32[16,64,4,64]{3,2,1,0:T(4,128)}, f32[16,64,4,128]{3,1,0,2:...) while((s32[]{:T(128)}, f32[4,128,64]{1,2,0:T(8,128)S(1)}, ...), condition=%wide.region_3.4_spmd, body=%wide.region_1.3_spmd.sunk | while | flops 253243456 | bytes 5288041 | solution.py:122
  53.7 19.7 %custom-call.6 = f32[4,1,64,64]{2,3,1,0:T(8,128)S(1)} custom-call(f32[4,1,64,64]{3,2,1,0:T(8,128)S(1)} %fusion.153), custom_call_target="InvertDiagBlocksLowerTriangular" | custom-call | tf_op jit(solution)/shard_map/while/body/eval_jaxpr/jit(_solve_triangular)/vmap()/triangular_solve | solution.py:75
  83.2 19.7 %custom-call.6 = f32[4,1,64,64]{2,3,1,0:T(8,128)S(1)} custom-call(f32[4,1,64,64]{3,2,1,0:T(8,128)S(1)} %fusion.153), custom_call_target="InvertDiagBlocksLowerTriangular" | custom-call | tf_op jit(solution)/shard_map/while/body/eval_jaxpr/jit(_solve_triangular)/vmap()/triangular_solve | solution.py:75
  112.7 19.7 %custom-call.6 = f32[4,1,64,64]{2,3,1,0:T(8,128)S(1)} custom-call(f32[4,1,64,64]{3,2,1,0:T(8,128)S(1)} %fusion.153), custom_call_target="InvertDiagBlocksLowerTriangular" | custom-call | tf_op jit(solution)/shard_map/while/body/eval_jaxpr/jit(_solve_triangular)/vmap()/triangular_solve | solution.py:75
  142.2 19.7 %custom-call.6 = f32[4,1,64,64]{2,3,1,0:T(8,128)S(1)} custom-call(f32[4,1,64,64]{3,2,1,0:T(8,128)S(1)} %fusion.153), custom_call_target="InvertDiagBlocksLowerTriangular" | custom-call | tf_op jit(solution)/shard_map/while/body/eval_jaxpr/jit(_solve_triangular)/vmap()/triangular_solve | solution.py:75
  171.7 19.7 %custom-call.6 = f32[4,1,64,64]{2,3,1,0:T(8,128)S(1)} custom-call(f32[4,1,64,64]{3,2,1,0:T(8,128)S(1)} %fusion.153), custom_call_target="InvertDiagBlocksLowerTriangular" | custom-call | tf_op jit(solution)/shard_map/while/body/eval_jaxpr/jit(_solve_triangular)/vmap()/triangular_solve | solution.py:75
  201.2 19.7 %custom-call.6 = f32[4,1,64,64]{2,3,1,0:T(8,128)S(1)} custom-call(f32[4,1,64,64]{3,2,1,0:T(8,128)S(1)} %fusion.153), custom_call_target="InvertDiagBlocksLowerTriangular" | custom-call | tf_op jit(solution)/shard_map/while/body/eval_jaxpr/jit(_solve_triangular)/vmap()/triangular_solve | solution.py:75
  230.7 19.7 %custom-call.6 = f32[4,1,64,64]{2,3,1,0:T(8,128)S(1)} custom-call(f32[4,1,64,64]{3,2,1,0:T(8,128)S(1)} %fusion.153), custom_call_target="InvertDiagBlocksLowerTriangular" | custom-call | tf_op jit(solution)/shard_map/while/body/eval_jaxpr/jit(_solve_triangular)/vmap()/triangular_solve | solution.py:75
  260.2 19.7 %custom-call.6 = f32[4,1,64,64]{2,3,1,0:T(8,128)S(1)} custom-call(f32[4,1,64,64]{3,2,1,0:T(8,128)S(1)} %fusion.153), custom_call_target="InvertDiagBlocksLowerTriangular" | custom-call | tf_op jit(solution)/shard_map/while/body/eval_jaxpr/jit(_solve_triangular)/vmap()/triangular_solve | solution.py:75
  289.7 19.7 %custom-call.6 = f32[4,1,64,64]{2,3,1,0:T(8,128)S(1)} custom-call(f32[4,1,64,64]{3,2,1,0:T(8,128)S(1)} %fusion.153), custom_call_target="InvertDiagBlocksLowerTriangular" | custom-call | tf_op jit(solution)/shard_map/while/body/eval_jaxpr/jit(_solve_triangular)/vmap()/triangular_solve | solution.py:75
  319.2 19.7 %custom-call.6 = f32[4,1,64,64]{2,3,1,0:T(8,128)S(1)} custom-call(f32[4,1,64,64]{3,2,1,0:T(8,128)S(1)} %fusion.153), custom_call_target="InvertDiagBlocksLowerTriangular" | custom-call | tf_op jit(solution)/shard_map/while/body/eval_jaxpr/jit(_solve_triangular)/vmap()/triangular_solve | solution.py:75
  348.7 19.7 %custom-call.6 = f32[4,1,64,64]{2,3,1,0:T(8,128)S(1)} custom-call(f32[4,1,64,64]{3,2,1,0:T(8,128)S(1)} %fusion.153), custom_call_target="InvertDiagBlocksLowerTriangular" | custom-call | tf_op jit(solution)/shard_map/while/body/eval_jaxpr/jit(_solve_triangular)/vmap()/triangular_solve | solution.py:75
  378.1 19.7 %custom-call.6 = f32[4,1,64,64]{2,3,1,0:T(8,128)S(1)} custom-call(f32[4,1,64,64]{3,2,1,0:T(8,128)S(1)} %fusion.153), custom_call_target="InvertDiagBlocksLowerTriangular" | custom-call | tf_op jit(solution)/shard_map/while/body/eval_jaxpr/jit(_solve_triangular)/vmap()/triangular_solve | solution.py:75
  407.6 19.7 %custom-call.6 = f32[4,1,64,64]{2,3,1,0:T(8,128)S(1)} custom-call(f32[4,1,64,64]{3,2,1,0:T(8,128)S(1)} %fusion.153), custom_call_target="InvertDiagBlocksLowerTriangular" | custom-call | tf_op jit(solution)/shard_map/while/body/eval_jaxpr/jit(_solve_triangular)/vmap()/triangular_solve | solution.py:75
  437.1 19.7 %custom-call.6 = f32[4,1,64,64]{2,3,1,0:T(8,128)S(1)} custom-call(f32[4,1,64,64]{3,2,1,0:T(8,128)S(1)} %fusion.153), custom_call_target="InvertDiagBlocksLowerTriangular" | custom-call | tf_op jit(solution)/shard_map/while/body/eval_jaxpr/jit(_solve_triangular)/vmap()/triangular_solve | solution.py:75
  521.1 35.6 %all-gather = bf16[32,64,64]{2,1,0:T(8,128)(2,1)} all-gather(bf16[4,64,64]{2,1,0:T(8,128)(2,1)S(1)} %get-tuple-element.184), channel_id=2, replica_groups=mesh['sp'=8,'tp'=4] {'sp'}, dimensions={0}, use_global_device_ids=true | all-gather | bytes 294912 | tf_op jit(solution)/shard_map/all_gather | solution.py:15
  556.7 33.4 %all-gather.1 = bf16[32,64,64]{2,1,0:T(8,128)(2,1)} all-gather(bf16[4,64,64]{2,1,0:T(8,128)(2,1)S(1)} %get-tuple-element.183), channel_id=3, replica_groups=mesh['sp'=8,'tp'=4] {'sp'}, dimensions={0}, use_global_device_ids=true | all-gather | bytes 294912 | tf_op jit(solution)/shard_map/all_gather | solution.py:15
  601.3 60.0 %reduce-scatter.3.cloned.1.call-done = bf16[256,2048]{1,0:T(8,128)(2,1)} async-done(((bf16[1024,2048]{1,0:T(8,128)(2,1)}), bf16[256,2048]{1,0:T(8,128)(2,1)}) %reduce-scatter.3.cloned.1.call-update) | async-done | bytes 1048592 | tf_op jit(solution)/shard_map/reduce_scatter | solution.py:198
  666.0 45.4 %all-gather.9.cloned.1.call-done = bf16[2048,1408]{1,0:T(8,128)(2,1)} async-done(((bf16[256,1408]{1,0:T(8,128)(2,1)}), bf16[2048,1408]{1,0:T(8,128)(2,1)}) %all-gather.9.cloned.1.call-update) | async-done | bytes 5767184 | tf_op jit(solution)/shard_map/all_gather | solution.py:166
  711.4 33.9 %all-gather.7.cloned.1.call-done = bf16[1024,2048]{1,0:T(8,128)(2,1)} async-done(((bf16[256,2048]{1,0:T(8,128)(2,1)}), bf16[1024,2048]{1,0:T(8,128)(2,1)}) %all-gather.7.cloned.1.call-update) | async-done | bytes 4194320 | tf_op jit(solution)/shard_map/all_gather | solution.py:215
  760.5 79.2 %all-gather.11.cloned.1.call-done = bf16[2048,1408]{1,0:T(8,128)(2,1)} async-done(((bf16[256,1408]{1,0:T(8,128)(2,1)}), bf16[2048,1408]{1,0:T(8,128)(2,1)}) %all-gather.11.cloned.1.call-update) | async-done | bytes 5767184 | tf_op jit(solution)/shard_map/all_gather | solution.py:167
  858.6 73.7 %all-gather.13.cloned.1.call-done = bf16[2048,1408]{1,0:T(8,128)(2,1)} async-done(((bf16[256,1408]{1,0:T(8,128)(2,1)}), bf16[2048,1408]{1,0:T(8,128)(2,1)}) %all-gather.13.cloned.1.call-update) | async-done | bytes 5767184 | tf_op jit(solution)/shard_map/all_gather | solution.py:168
  932.3 23.1 %convolution_convert_fusion.2 = bf16[1024,2048]{1,0:T(8,128)(2,1)} fusion(bf16[2048,1408]{1,0:T(8,128)(2,1)} %all-gather.13.cloned.1.call-done, f32[1026,1408]{1,0:T(8,128)} %maximum_convert_fusion.1, f32[1026,1408]{1,0:T(8,128)} %maximum_convert_fusion, f32[1408]{0:T(1024)S(1)} %get-tuple-element.124, f32[1408]{0:T(1024)S(1)} %get-tuple-element.125, ...), kind=kOutput, calls=%fused_computation.89 | convolution fusion | flops 5930745856 | bytes 44598272 | tf_op jit(solution)/shard_map/dot_general | solution.py:226
  955.4 42.9 %reduce-scatter.5.cloned.1.call-done = bf16[256,2048]{1,0:T(8,128)(2,1)} async-done(((bf16[1024,2048]{1,0:T(8,128)(2,1)}), bf16[256,2048]{1,0:T(8,128)(2,1)}) %reduce-scatter.5.cloned.1.call-update) | async-done | bytes 1048592 | tf_op jit(solution)/shard_map/reduce_scatter | solution.py:225
  (404 shorter events, 288.7 us)
Async XLA Ops:
  7.4 589.1 %copy-start = (bf16[256,2048]{1,0:T(8,128)(2,1)S(1)}, bf16[256,2048]{1,0:T(8,128)(2,1)}, u32[]{:S(2)}) copy-start(bf16[256,2048]{1,0:T(8,128)(2,1)} %param.28) | copy-start | bytes 3145732
  7.4 653.9 %reduce-scatter.3.cloned.1.call-start = ((), (), s32[]{:S(2)}) async-start(), calls=%async_computation.2 | async-start | bytes 5242880 | tf_op jit(solution)/shard_map/reduce_scatter | solution.py:198
  38.5 6.7 copy-start.5
  521.1 69.1 %copy-start.2 = (f32[16,64,4,128]{3,1,0,2:T(8,128)S(1)}, f32[16,64,4,128]{3,1,0,2:T(8,128)}, u32[]{:S(2)}) copy-start(f32[16,64,4,128]{3,1,0,2:T(8,128)} %get-tuple-element.97) | copy-start | bytes 6291460
  595.8 0.7 copy-start.9
  600.7 60.6 %copy-start.6 = (bf16[256,2048]{1,0:T(8,128)(2,1)S(1)}, bf16[256,2048]{1,0:T(8,128)(2,1)}, u32[]{:S(2)}) copy-start(bf16[256,2048]{1,0:T(8,128)(2,1)} %param.19) | copy-start | bytes 3145732
  600.7 62.5 %copy-start.8 = (f32[2048]{0:T(1024)S(1)}, f32[2048]{0:T(1024)}, u32[]{:S(2)}) copy-start(f32[2048]{0:T(1024)} %param.29) | copy-start | bytes 24580
  600.7 110.7 %all-gather.9.cloned.1.call-start = ((), (), s32[]{:S(2)}) async-start(), calls=%async_computation.4 | async-start | bytes 6488064 | tf_op jit(solution)/shard_map/all_gather | solution.py:166
  601.3 144.1 %all-gather.7.cloned.1.call-start = ((), (), s32[]{:S(2)}) async-start(), calls=%async_computation.3 | async-start | bytes 5242880 | tf_op jit(solution)/shard_map/all_gather | solution.py:215
  662.9 3.0 copy-start.7
  664.5 175.1 %all-gather.11.cloned.1.call-start = ((), (), s32[]{:S(2)}) async-start(), calls=%async_computation.5 | async-start | bytes 6488064 | tf_op jit(solution)/shard_map/all_gather | solution.py:167
  665.1 267.2 %all-gather.13.cloned.1.call-start = ((), (), s32[]{:S(2)}) async-start(), calls=%async_computation.6 | async-start | bytes 6488064 | tf_op jit(solution)/shard_map/all_gather | solution.py:168
  665.9 332.4 %reduce-scatter.5.cloned.1.call-start = ((), (), s32[]{:S(2)}) async-start(), calls=%async_computation.7 | async-start | bytes 5242880 | tf_op jit(solution)/shard_map/reduce_scatter | solution.py:225
  755.5 1.6 copy-start.3
  757.1 95.4 %collective-permute-start = (bf16[2,1408]{1,0:T(2,128)(2,1)S(1)}, bf16[2,1408]{1,0:T(2,128)(2,1)S(1)}, u32[]{:S(2)}, u32[]{:S(2)}) collective-permute-start(bf16[2,1408]{1,0:T(2,128)(2,1)S(1)} %slice.108), channel_id=1, source_target_pairs={{0,4},{4,8},{8,12},{12,16},{16,20},{20,24},{24,28},{1,5},{5,9},{9,... | collective-permute-start | bytes 16904 | tf_op jit(solution)/shard_map/ppermute | solution.py:35
  839.7 12.8 %copy-start.4 = (bf16[1024,1408]{1,0:T(8,128)(2,1)S(1)}, bf16[1024,1408]{1,0:T(8,128)(2,1)}, u32[]{:S(2)}) copy-start(bf16[1024,1408]{1,0:T(8,128)(2,1)} %copy-done.3) | copy-start | bytes 8650756
  850.0 5.5 collective-permute-start.1
  955.4 45.5 %copy-start.1 = (bf16[256,2048]{1,0:T(8,128)(2,1)S(1)}, bf16[256,2048]{1,0:T(8,128)(2,1)}, u32[]{:S(2)}) copy-start(bf16[256,2048]{1,0:T(8,128)(2,1)} %param.28) | copy-start | bytes 3145732
Sparse Core Ops, SparseCore 0:
  600.8 60.4 reduce-scatter.2
  955.5 42.7 reduce-scatter.4
Sparse Core Ops, SparseCore 1:
  603.4 108.0 all-gather.8
  712.9 32.4 all-gather.6
  747.4 92.2 all-gather.10
  841.9 90.4 all-gather.12
where the time goes:
time: 1010 us
  other arithmetic  385 us (38%)
  waiting for transfers between devices  337 us (33%)
  matrix products  167 us (17%)
  blocking collectives  69 us (7%)
  local copies, waits for them, and re-layouts  26.8 us (3%)
  between operations  15.4 us (2%)
    another operation x32, other arithmetic, block_step(): jax.scipy.linalg.solve_triangular(unit_lower, right_side, lower=True, uni...  315 us
    all_gather x1, waiting for transfers between devices, body(): lax.all_gather(up_projection_weight, 'sp', axis=0, tiled=True)  79.2 us
    all_gather x1, waiting for transfers between devices, body(): lax.all_gather(down_projection_weight, 'sp', axis=0, tiled=True)  73.7 us
    all_gather x2, blocking collectives, entering(): lax.all_gather(a.astype(kind), axis)  69 us
    reduce_scatter x1, waiting for transfers between devices, body(): lax.psum_scatter(jnp.dot(mixed_out, output_projection_weight, preferred_e...  60 us
    all_gather x1, waiting for transfers between devices, body(): lax.all_gather(gate_projection_weight, 'sp', axis=0, tiled=True)  45.4 us
    reduce_scatter x1, waiting for transfers between devices, body(): lax.psum_scatter(lax.dot_general(hidden, full_down, (((1,), (1,)), ((), (...  42.9 us
    all_gather x1, waiting for transfers between devices, body(): whole_rows = lax.all_gather(normed, 'tp', axis=0, tiled=True)  33.9 us
  transfers between devices with their start and end apart: 8, of which 6 were waited for; matrix products, arithmetic and copies ran while one was open for 3% of the time, Pallas kernels for 0%

commit v1 on v0

v1 whole, which is shorter than its diff:
```python
import functools

import jax
import jax.numpy as jnp
from jax import lax
from jax.experimental import pallas as pl
from jax.experimental.pallas import tpu as pltpu
from jax.sharding import PartitionSpec as P

HEAD_WIDTH = 64
BLOCK = 64
PER_STEP = 4
PIECES = 4
MESH = pl.DeviceIdType.MESH
WIDE = jnp.float32
NARROW = jnp.bfloat16


def mul(a, b, dims=((1,), (0,))):
    return lax.dot_general(
        a.astype(NARROW), b.astype(NARROW), (dims, ((), ())), preferred_element_type=WIDE
    )


def parts_of(a, count):
    found = []
    for _ in range(count):
        piece = a.astype(NARROW)
        found.append(piece)
        a = a - piece.astype(WIDE)
    return found


def fine_left(a, b, count, dims=((1,), (0,))):
    return sum(mul(piece, b, dims) for piece in parts_of(a, count))


def fine_right(a, b, count, dims=((1,), (0,))):
    return sum(mul(a, piece, dims) for piece in parts_of(b, count))


def head_mask(width):
    rows = lax.broadcasted_iota(jnp.int32, (width, width), 0) // HEAD_WIDTH
    lanes = lax.broadcasted_iota(jnp.int32, (width, width), 1) // HEAD_WIDTH
    return jnp.where(rows == lanes, 1.0, 0.0)


def stacked(a, mask):
    a = a.astype(NARROW)
    return jnp.concatenate([a] * (mask.shape[0] // a.shape[0]), axis=0) * mask


def fine_product(a, b, mask):
    a_high, a_low = parts_of(a, 2)
    b_high, b_low = (stacked(piece, mask) for piece in parts_of(b, 2))
    return mul(a_high, b_high) + mul(a_low, b_high) + mul(a_high, b_low)


def collapsed(a):
    heads = a.shape[0] // HEAD_WIDTH
    return sum(a[h * HEAD_WIDTH : (h + 1) * HEAD_WIDTH] for h in range(heads))


def recurrence_kernel(
    q_ref, k_ref, v_ref, decay_ref, rate_ref, extra_ref, local_ref, reach_ref, map_ref, state
):
    width = q_ref.shape[1]
    mask_wide = head_mask(width)
    mask = mask_wide.astype(NARROW)
    last = ((1,), (1,))
    first = ((0,), (0,))

    @pl.when(pl.program_id(0) == 0)
    def _():
        rows = lax.broadcasted_iota(jnp.int32, (width, width), 0)
        lanes = lax.broadcasted_iota(jnp.int32, (width, width), 1)
        state[:, :width] = jnp.zeros((width, width), WIDE)
        state[:, width:] = jnp.where(rows == lanes, 1.0, 0.0)

    token = lax.broadcasted_iota(jnp.int32, (BLOCK, width), 0)
    other = lax.broadcasted_iota(jnp.int32, (BLOCK, width), 1) % BLOCK
    strict = token > other
    within = token >= other
    eye = jnp.where(token == other, 1.0, 0.0)
    lower = jnp.where(
        lax.broadcasted_iota(jnp.int32, (BLOCK, BLOCK), 0)
        >= lax.broadcasted_iota(jnp.int32, (BLOCK, BLOCK), 1),
        1.0,
        0.0,
    ).astype(NARROW)
    ones = jnp.ones((BLOCK, width), NARROW)

    prepared = []
    for part in range(PER_STEP):
        at = slice(part * BLOCK, (part + 1) * BLOCK)
        q = q_ref[at].astype(WIDE)
        k = k_ref[at].astype(WIDE)
        v = stacked(v_ref[at], mask)
        log_decay = (
            -jnp.exp(-0.5) * jax.nn.sigmoid(decay_ref[at].astype(WIDE)) + extra_ref[at]
        )
        rates = jax.nn.sigmoid(rate_ref[at].astype(WIDE))
        normed = k * lax.rsqrt(fine_left(k * k, mask, 2) + 1e-06)
        removal = normed * rates
        cum = fine_right(lower, log_decay, 3)
        previous = cum - log_decay
        middle = cum[BLOCK // 2 : BLOCK // 2 + 1]
        end = cum[BLOCK - 1 : BLOCK]
        back = jnp.exp(middle - cum)
        left = jnp.concatenate(
            [normed * jnp.exp(previous - middle), q * jnp.exp(cum - middle)], axis=0
        )
        by_key = mul(left, stacked(k * back, mask), last)
        by_removal = mul(left, stacked(removal * back, mask), last)
        key_rate = jnp.where(strict, by_key[:BLOCK], 0.0)
        removal_rate = jnp.where(strict, by_removal[:BLOCK], 0.0)
        key_out = jnp.where(within, by_key[BLOCK:], 0.0)
        removal_out = jnp.where(within, by_removal[BLOCK:], 0.0)
        inverse = eye
        size = 1
        while size < BLOCK:
            pair = (token // (2 * size) == other // (2 * size)) & (
                token // size != other // size
            )
            piece = jnp.where(pair, removal_rate, 0.0)
            if size == 1:
                inverse = inverse - piece
            else:
                inverse = inverse - fine_product(fine_product(inverse, piece, mask), inverse, mask)
            size *= 2
        from_state = mul(inverse, stacked(normed * jnp.exp(previous), mask))
        keyed = mul(jnp.concatenate([key_rate, key_out], axis=0), v)
        offset = mul(inverse, stacked(keyed[:BLOCK], mask))
        reach = q * jnp.exp(cum) - mul(removal_out, stacked(from_state, mask))
        local = keyed[BLOCK:] - mul(removal_out, stacked(offset, mask))
        to_end = jnp.exp(end - cum)
        span = jnp.exp(fine_left(log_decay, ones, 3, first))
        prepared.append((from_state, offset, reach, local, k * to_end, removal * to_end, span))

    for part in range(PER_STEP):
        at = slice(part * BLOCK, (part + 1) * BLOCK)
        from_state, offset, reach, local, key_end, removal_end, span = prepared[part]
        now = state[...]
        both = mul(jnp.concatenate([from_state, reach], axis=0), now)
        correction = both[:BLOCK, :width] + offset
        local_ref[at] = local + both[BLOCK:, :width]
        reach_ref[at] = both[BLOCK:, width:]
        kept_value = mul(
            jnp.concatenate([key_end, -removal_end], axis=0),
            jnp.concatenate([v_ref[at].astype(WIDE), correction], axis=0),
            first,
        )
        kept_map = mul(-removal_end, both[:BLOCK, width:], first)
        state[:, :width] = now[:, :width] * span + kept_value * mask_wide
        state[:, width:] = now[:, width:] * span + kept_map * mask_wide

    @pl.when(pl.program_id(0) == pl.num_programs(0) - 1)
    def _():
        map_ref[...] = collapsed(state[...]).astype(NARROW)


def recurrence(q, k, v, decay, rate, extra):
    tokens, width = q.shape
    rows = BLOCK * PER_STEP
    spec = pl.BlockSpec((rows, width), lambda i: (i, 0))
    return pl.pallas_call(
        recurrence_kernel,
        grid=(tokens // rows,),
        in_specs=[spec] * 6,
        out_specs=[spec, spec, pl.BlockSpec((HEAD_WIDTH, 2 * width), lambda i: (0, 0))],
        out_shape=[
            jax.ShapeDtypeStruct((tokens, width), WIDE),
            jax.ShapeDtypeStruct((tokens, width), WIDE),
            jax.ShapeDtypeStruct((HEAD_WIDTH, 2 * width), NARROW),
        ],
        scratch_shapes=[pltpu.VMEM((width, 2 * width), WIDE)],
        compiler_params=pltpu.CompilerParams(
            dimension_semantics=("arbitrary",), vmem_limit_bytes=40 * 1024 * 1024
        ),
        cost_estimate=pl.CostEstimate(
            flops=250 * tokens * width * width * 2, bytes_accessed=8 * tokens * width * 2,
            transcendentals=0,
        ),
        name="recurrence",
    )(q, k, v, decay, rate, extra)


def exchange_kernel(axis, x_ref, o_ref, send_sem, recv_sem, local_sem):
    count = lax.axis_size(axis)
    me = lax.axis_index(axis)
    barrier = pltpu.get_barrier_semaphore()
    for step in range(1, count):
        pl.semaphore_signal(
            barrier, inc=1, device_id={axis: lax.rem(me + step, count)}, device_id_type=MESH
        )
    pl.semaphore_wait(barrier, count - 1)
    own = pltpu.make_async_copy(x_ref, o_ref.at[me], local_sem)
    own.start()
    copies = []
    for step in range(1, count):
        copy = pltpu.make_async_remote_copy(
            src_ref=x_ref,
            dst_ref=o_ref.at[me],
            send_sem=send_sem.at[step - 1],
            recv_sem=recv_sem.at[step - 1],
            device_id={axis: lax.rem(me + step, count)},
            device_id_type=MESH,
        )
        copy.start()
        copies.append(copy)
    own.wait()
    for copy in copies:
        copy.wait()


def exchange(x, axis, identity):
    count = lax.axis_size(axis)
    return pl.pallas_call(
        functools.partial(exchange_kernel, axis),
        out_shape=jax.ShapeDtypeStruct((count,) + x.shape, x.dtype),
        in_specs=[pl.BlockSpec(memory_space=pltpu.VMEM)],
        out_specs=pl.BlockSpec(memory_space=pltpu.VMEM),
        scratch_shapes=[
            pltpu.SemaphoreType.DMA((count - 1,)),
            pltpu.SemaphoreType.DMA((count - 1,)),
            pltpu.SemaphoreType.DMA,
        ],
        compiler_params=pltpu.CompilerParams(collective_id=identity, has_side_effects=True),
        name="exchange",
    )(x)


def pieces_of(axis, rows):
    count = lax.axis_size(axis)
    me = lax.axis_index(axis)
    half = count // 2
    pair = me // 2
    side = lax.rem(me, 2)
    step = rows // PIECES

    def device(offset, sibling):
        group = lax.rem(pair + offset + half, half)
        return 2 * group + (1 - side if sibling else side)

    def window(owner, piece):
        return pl.ds(pl.multiple_of(owner * rows + piece * step, step), step)

    return half, device, window, step


def greet(axis):
    count = lax.axis_size(axis)
    me = lax.axis_index(axis)
    barrier = pltpu.get_barrier_semaphore()
    for step in range(1, count):
        pl.semaphore_signal(
            barrier, inc=1, device_id={axis: lax.rem(me + step, count)}, device_id_type=MESH
        )
    pl.semaphore_wait(barrier, count - 1)


def send(axis, source, target, sems, index, device):
    copy = pltpu.make_async_remote_copy(
        src_ref=source,
        dst_ref=target,
        send_sem=sems[0].at[index],
        recv_sem=sems[1].at[index],
        device_id={axis: device},
        device_id_type=MESH,
    )
    copy.start()
    return copy


def summed_pieces(axis, partial, near, leaving, far, near_sems, far_sems, finish):
    rows = near.shape[1]
    half, device, window, step = pieces_of(axis, rows)
    order = list(range(1, half)) + [0]
    near_copies = {}
    for offset in order:
        for piece in range(PIECES):
            near_copies[offset, piece] = send(
                axis,
                partial.at[window(device(offset, True), piece)],
                near.at[offset, pl.ds(piece * step, step)],
                near_sems,
                offset * PIECES + piece,
                device(0, True),
            )
    far_copies = {}
    for piece in range(PIECES):
        at = pl.ds(piece * step, step)
        for offset in range(1, half):
            near_copies[offset, piece].wait_recv()
            mine = partial[window(device(offset, False), piece)].astype(WIDE)
            leaving[offset - 1, at] = (mine + near[offset, at].astype(WIDE)).astype(NARROW)
            far_copies[offset, piece] = send(
                axis,
                leaving.at[offset - 1, at],
                far.at[offset - 1, at],
                far_sems,
                (offset - 1) * PIECES + piece,
                device(offset, False),
            )
    for piece in range(PIECES):
        at = pl.ds(piece * step, step)
        near_copies[0, piece].wait_recv()
        total = partial[window(device(0, False), piece)].astype(WIDE) + near[0, at].astype(WIDE)
        for offset in range(1, half):
            far_copies[offset, piece].wait_recv()
            total = total + far[offset - 1, at].astype(WIDE)
        finish(piece, at, total)
    for copy in list(near_copies.values()) + list(far_copies.values()):
        copy.wait_send()


def stream_kernel(
    axis, partial, residual, gain, stream, whole, near, leaving, far,
    near_send, near_recv, far_send, far_recv, side_send, side_recv, out_send, out_recv,
    pass_send, pass_recv,
):
    greet(axis)
    half, device, window, _ = pieces_of(axis, residual.shape[0])
    side_copies = {}
    out_copies = {}
    pass_copies = {}

    def finish(piece, at, total):
        kept = (residual[at].astype(WIDE) + total).astype(NARROW)
        stream[at] = kept
        kept = kept.astype(WIDE)
        scale = lax.rsqrt(jnp.mean(kept * kept, axis=-1, keepdims=True) + 1e-06)
        own = window(device(0, False), piece)
        whole[own] = (kept * scale * gain[...]).astype(NARROW)
        for offset in range(1, half):
            out_copies[offset, piece] = send(
                axis, whole.at[own], whole.at[own], (out_send, out_recv),
                (offset - 1) * PIECES + piece, device(offset, False),
            )
        side_copies[piece] = send(
            axis, whole.at[own], whole.at[own], (side_send, side_recv), piece, device(0, True)
        )

    summed_pieces(
        axis, partial, near, leaving, far, (near_send, near_recv), (far_send, far_recv), finish
    )
    for piece in range(PIECES):
        for offset in range(1, half):
            out_copies[offset, piece].wait_recv()
            arrived = window(device(-offset, False), piece)
            pass_copies[offset, piece] = send(
                axis, whole.at[arrived], whole.at[arrived], (pass_send, pass_recv),
                (offset - 1) * PIECES + piece, device(0, True),
            )
    for copy in list(out_copies.values()):
        copy.wait_send()
    for copy in list(side_copies.values()) + list(pass_copies.values()):
        copy.wait()


def closing_kernel(
    axis, partial, stream, out, near, leaving, far, near_send, near_recv, far_send, far_recv
):
    greet(axis)

    def finish(piece, at, total):
        out[at] = (stream[at].astype(WIDE) + total).astype(NARROW)

    summed_pieces(
        axis, partial, near, leaving, far, (near_send, near_recv), (far_send, far_recv), finish
    )


def sum_scratch(axis, rows, features):
    half = lax.axis_size(axis) // 2
    dma = pltpu.SemaphoreType.DMA
    others = (half - 1) * PIECES
    return [
        pltpu.VMEM((half, rows, features), NARROW),
        pltpu.VMEM((half - 1, rows, features), NARROW),
        pltpu.VMEM((half - 1, rows, features), NARROW),
        dma((half * PIECES,)),
        dma((half * PIECES,)),
        dma((others,)),
        dma((others,)),
    ]


def streamed(partial, residual, gain, axis, identity):
    rows, features = residual.shape
    dma = pltpu.SemaphoreType.DMA
    others = (lax.axis_size(axis) // 2 - 1) * PIECES
    in_vmem = pl.BlockSpec(memory_space=pltpu.VMEM)
    return pl.pallas_call(
        functools.partial(stream_kernel, axis),
        in_specs=[in_vmem] * 3,
        out_specs=[in_vmem] * 2,
        out_shape=[
            jax.ShapeDtypeStruct((rows, features), NARROW),
            jax.ShapeDtypeStruct(partial.shape, NARROW),
        ],
        scratch_shapes=sum_scratch(axis, rows, features)
        + [dma((PIECES,)), dma((PIECES,))]
        + [dma((others,))] * 4,
        compiler_params=pltpu.CompilerParams(
            collective_id=identity, has_side_effects=True, vmem_limit_bytes=40 * 1024 * 1024
        ),
        name="streamed",
    )(partial, residual, gain[None])


def closed(partial, stream, axis, identity):
    rows, features = stream.shape
    in_vmem = pl.BlockSpec(memory_space=pltpu.VMEM)
    return pl.pallas_call(
        functools.partial(closing_kernel, axis),
        in_specs=[in_vmem] * 2,
        out_specs=in_vmem,
        out_shape=jax.ShapeDtypeStruct((rows, features), NARROW),
        scratch_shapes=sum_scratch(axis, rows, features),
        compiler_params=pltpu.CompilerParams(
            collective_id=identity, has_side_effects=True, vmem_limit_bytes=40 * 1024 * 1024
        ),
        name="closed",
    )(partial, stream)


def project_kernel(local_ref, reach_ref, maps_ref, gain_ref, gate_ref, weight_ref, out_ref, state):
    width = local_ref.shape[1]
    mask = head_mask(width).astype(NARROW)

    @pl.when(pl.program_id(0) == 0)
    def _():
        place = lax.axis_index("sp")

        def one(step, entering):
            maps = maps_ref[step]
            high, low = parts_of(entering, 2)
            after = (
                maps[:, :width].astype(WIDE)
                + mul(maps[:, width:], stacked(high, mask))
                + mul(maps[:, width:], stacked(low, mask))
            )
            return jnp.where(step < place, after, entering)

        state[...] = lax.fori_loop(
            0, maps_ref.shape[0] - 1, one, jnp.zeros((HEAD_WIDTH, width), WIDE)
        )

    readout = local_ref[...] + mul(reach_ref[...], stacked(state[...], mask))
    centered = readout - fine_left(readout, mask, 2) * (1.0 / HEAD_WIDTH)
    variance = fine_left(centered * centered, mask, 2) * (1.0 / HEAD_WIDTH)
    mixed = (
        centered * lax.rsqrt(variance + 0.00064) * gain_ref[...] * gate_ref[...].astype(WIDE)
    )
    out_ref[...] = mul(mixed, weight_ref[...]).astype(NARROW)


def project(local, reach, maps, gain, gate, weight):
    tokens, width = local.shape
    rows = 256
    spec = pl.BlockSpec((rows, width), lambda i: (i, 0))
    features = weight.shape[1]
    return pl.pallas_call(
        project_kernel,
        grid=(tokens // rows,),
        in_specs=[
            spec,
            spec,
            pl.BlockSpec(maps.shape, lambda i: (0, 0, 0)),
            pl.BlockSpec((1, width), lambda i: (0, 0)),
            spec,
            pl.BlockSpec(weight.shape, lambda i: (0, 0)),
        ],
        out_specs=pl.BlockSpec((rows, features), lambda i: (i, 0)),
        out_shape=jax.ShapeDtypeStruct((tokens, features), NARROW),
        scratch_shapes=[pltpu.VMEM((HEAD_WIDTH, width), WIDE)],
        compiler_params=pltpu.CompilerParams(
            dimension_semantics=("arbitrary",), vmem_limit_bytes=40 * 1024 * 1024
        ),
        name="project",
    )(local, reach, maps, gain[None], gate, weight)


def passed_along(x, axis, by):
    count = lax.axis_size(axis)
    pairs = [(i, i + by) for i in range(count) if 0 <= i + by < count]
    return lax.ppermute(x, axis, pairs)


def conv_mix(before_rows, current, taps):
    extended = jnp.concatenate([before_rows, current], axis=0).astype(jnp.float32)
    return taps[0] * extended[:-2] + taps[1] * extended[1:-1] + taps[2] * extended[2:]


def body(
    residual_input_stream,
    receptance,
    key_matrix_all,
    value_matrix_all,
    decay_preactivation,
    learning_rate_preactivation,
    output_gate_all_heads,
    extra_log_decay,
    head_norm_gain,
    output_projection_weight,
    feedforward_norm_gain,
    gate_projection_weight,
    up_projection_weight,
    down_projection_weight,
    convolution_kernel,
):
    full_gate = lax.all_gather(gate_projection_weight, "sp", axis=0, tiled=True)
    full_up = lax.all_gather(up_projection_weight, "sp", axis=0, tiled=True)
    full_down = lax.all_gather(down_projection_weight, "sp", axis=0, tiled=True)
    local, reach, own_map = recurrence(
        receptance,
        key_matrix_all,
        value_matrix_all,
        decay_preactivation,
        learning_rate_preactivation,
        extra_log_decay,
    )
    maps = exchange(own_map, "sp", 1)
    partial = project(
        local, reach, maps, head_norm_gain, output_gate_all_heads, output_projection_weight
    )
    stream, whole_rows = streamed(
        partial, residual_input_stream, feedforward_norm_gain, "tp", 2
    )
    gate_acc = jnp.dot(whole_rows, full_gate, preferred_element_type=jnp.float32)
    up_acc = jnp.dot(whole_rows, full_up, preferred_element_type=jnp.float32)
    gate_pre = gate_acc.astype(jnp.bfloat16)
    up_pre = up_acc.astype(jnp.bfloat16)
    before = passed_along((gate_pre[-2:], up_pre[-2:]), "sp", 1)
    taps = convolution_kernel.astype(jnp.float32)
    gate_mix = conv_mix(before[0], gate_pre, taps[:, 0])
    up_mix = conv_mix(before[1], up_pre, taps[:, 1])
    hidden = (jax.nn.silu(gate_mix) * up_mix).astype(jnp.bfloat16)
    ffn_part = lax.dot_general(
        hidden, full_down, (((1,), (1,)), ((), ())), preferred_element_type=jnp.float32
    ).astype(jnp.bfloat16)
    return closed(ffn_part, stream, "tp", 3)


def solution(mesh):
    in_specs = (
        P(("sp", "tp"), None),
        P("sp", "tp"),
        P("sp", "tp"),
        P("sp", "tp"),
        P("sp", "tp"),
        P("sp", "tp"),
        P("sp", "tp"),
        P("sp", "tp"),
        P("tp"),
        P("tp", None),
        P(),
        P("sp", "tp"),
        P("sp", "tp"),
        P("sp", "tp"),
        P(None, None, "tp"),
    )
    out_specs = P(("sp", "tp"), None)
    return jax.shard_map(body, mesh=mesh, in_specs=in_specs, out_specs=out_specs, check_vma=False)
```

time: 1010 us -> 360 us (0.36)
  other arithmetic: 385 us -> 6.18 us
  waiting for transfers between devices: 337 us -> 116 us
  Pallas kernels: 0 us -> 158 us
  matrix products: 167 us -> 43.7 us
  blocking collectives: 69 us -> 0 us
    another operation x48 -> x0, other arithmetic: 330 us -> none  [the longest x32 315 us: block_step(): jax.scipy.linalg.solve_triangular(unit_lower, right_side, lower=True, uni...]
    pallas_call x0 -> x5, Pallas kernels: none -> 158 us  [the longest x1 51 us: streamed(): pl.pallas_call(functools.partial(stream_kernel, axis), in_specs=[in_vmem]...]
    all_gather x4 -> x3, waiting for transfers between devices: 232 us -> 114 us  [the longest x1 73.9 us: body(): full_down = lax.all_gather(down_projection_weight, 'sp', axis=0, tiled=True)]
    dot_general x178 -> x0, matrix products: 118 us -> none  [the longest x16 20.7 us: block_step(): jnp.einsum('shr,shk->hrk', values_aug, keys * to_end, precision=highest)]
    reduce_scatter x2 -> x0, waiting for transfers between devices: 103 us -> none  [the longest x1 60 us: body(): lax.psum_scatter(jnp.dot(mixed_out, output_projection_weight, preferred_e...]
    all_gather x2 -> x0, blocking collectives: 69 us -> none  [entering(): lax.all_gather(a.astype(kind), axis)]
    mul x18 -> x0, other arithmetic: 26.5 us -> none  [the longest x16 22.5 us: block_step(): scaled_normed = normed_keys * jnp.exp(previous - middle)]
    unnamed x23 -> x41, local copies, waits for them, and re-layouts: 7.35 us -> 18.1 us
  transfers between devices with their start and end apart: 8 -> 5, of which waited for: 6 -> 2; matrix products, arithmetic and copies ran while one was open for 3% -> 8% of each run, Pallas kernels for 0% -> 36%
where the time goes in v1:
time: 360 us
  Pallas kernels  158 us (44%)
  waiting for transfers between devices  116 us (32%)
  matrix products  43.7 us (12%)
  local copies, waits for them, and re-layouts  18.2 us (5%)
  between operations  13.3 us (4%)
  other arithmetic  6.18 us (2%)
  starting transfers between devices  4.49 us (1%)
    all_gather x1, waiting for transfers between devices, body(): full_down = lax.all_gather(down_projection_weight, 'sp', axis=0, tiled=True)  73.9 us
    pallas_call x1, Pallas kernels, streamed(): pl.pallas_call(functools.partial(stream_kernel, axis), in_specs=[in_vmem]...  51 us
    pallas_call x1, Pallas kernels, recurrence(): pl.pallas_call(recurrence_kernel, grid=(tokens // rows,), in_specs=[spec]...  48.9 us
    all_gather x1, waiting for transfers between devices, body(): full_up = lax.all_gather(up_projection_weight, 'sp', axis=0, tiled=True)  39.9 us
    pallas_call x1, Pallas kernels, closed(): pl.pallas_call(functools.partial(closing_kernel, axis), in_specs=[in_vmem...  27.3 us
    pallas_call x1, Pallas kernels, exchange(): pl.pallas_call(functools.partial(exchange_kernel, axis), out_shape=jax.Sh...  25.5 us
    dot_general x1, matrix products, body(): lax.dot_general(hidden, full_down, (((1,), (1,)), ((), ())), preferred_el...  22.6 us
    unnamed x41, local copies, waits for them, and re-layouts  18.1 us
  transfers between devices with their start and end apart: 5, of which 2 were waited for; matrix products, arithmetic and copies ran while one was open for 8% of the time, Pallas kernels for 36%

profile of v1, /device:TPU:0, one launch (start us, length us, event | category | flops | bytes accessed | tf_op | source)
XLA Modules:
  0.0 359.9 jit_solution(5394768280537171407)
XLA Ops:
  8.8 1.2 copy-done.11
  10.0 1.0 copy-done.12
  11.0 1.0 copy-done.13
  13.1 1.0 copy-done.15
  14.1 1.0 copy-done.16
  15.2 48.9 %recurrence.1 = (f32[1024,256]{1,0:T(8,128)S(1)}, f32[1024,256]{1,0:T(8,128)S(1)}, bf16[64,512]{1,0:T(8,128)(2,1)S(1)}) custom-call(bf16[1024,256]{1,0:T(8,128)(2,1)S(1)} %copy-done.12, bf16[1024,256]{1,0:T(8,128)(2,1)S(1)} %copy-done.13, bf16[1024,256]{1,0:T(8,128)(2,1)S(1)} %copy-done.14, bf16[1024,256]{1,0:T(8,128)(2,1)S(1)} %copy-done.15, ...), custom_call_target="tpu_custom_call" | custom-call | flops 33554432000 | bytes 4194304 | tf_op jit(solution)/shard_map/recurrence/pallas_call | solution.py:166
  65.7 25.5 %exchange.1.maps_ref = bf16[8,64,512]{2,1,0:T(8,128)(2,1)} custom-call(bf16[64,512]{1,0:T(8,128)(2,1)} %copy-done.7), custom_call_target="tpu_custom_call" | custom-call | tf_op jit(solution)/shard_map/exchange/pallas_call | solution.py:218
  92.3 1.3 copy-done.5
  93.5 1.0 copy-done.6
  94.6 5.4 %project.1.partial = bf16[1024,2048]{1,0:T(8,128)(2,1)S(1)} custom-call(f32[1024,256]{1,0:T(8,128)S(1)} %get-tuple-element.10.local_ref, f32[1024,256]{1,0:T(8,128)S(1)} %copy-done.5, bf16[8,64,512]{2,1,0:T(8,128)(2,1)S(1)} %copy-done.1, f32[1,256]{1,0:T(1,128)S(1)} %bitcast.8, bf16[1024,256]{1,0:T(8,128)(2,1)S(1)} %copy-done.6, bf16[256,2048]{1,0:T(8,128)(2,1)S(1)} %copy-done.2), custom_call_target="tpu_custom_call" | custom-call | tf_op jit(solution)/shard_map/project/pallas_call | solution.py:464
  100.0 51.0 %streamed.1 = (bf16[256,2048]{1,0:T(8,128)(2,1)S(1)}, bf16[1024,2048]{1,0:T(8,128)(2,1)S(1)}) custom-call(bf16[1024,2048]{1,0:T(8,128)(2,1)S(1)} %project.1.partial, bf16[256,2048]{1,0:T(8,128)(2,1)S(1)} %copy-done.3, f32[1,2048]{1,0:T(1,128)S(1)} %bitcast.7), custom_call_target="tpu_custom_call" | custom-call | tf_op jit(solution)/shard_map/streamed/pallas_call | solution.py:394
  151.0 2.0 copy-done.10
  153.1 10.8 %convolution_convert_fusion.1 = bf16[1024,1408]{1,0:T(8,128)(2,1)S(1)} fusion(bf16[1024,2048]{1,0:T(8,128)(2,1)} %copy-done.10, bf16[2048,1408]{1,0:T(8,128)(2,1)} %all-gather.4.cloned.1.call-done), kind=kOutput, calls=%fused_computation.13 | convolution fusion | flops 5907021824 | bytes 12845056 | tf_op jit(solution)/shard_map/dot_general | solution.py:531
  163.9 1.6 copy-done.17
  165.6 2.0 collective-permute-start
  167.5 39.9 %all-gather.6.cloned.1.call-done = bf16[2048,1408]{1,0:T(8,128)(2,1)} async-done(((bf16[256,1408]{1,0:T(8,128)(2,1)}), bf16[2048,1408]{1,0:T(8,128)(2,1)}) %all-gather.6.cloned.1.call-update) | async-done | bytes 5767184 | tf_op jit(solution)/shard_map/all_gather | solution.py:514
  207.5 10.3 %convolution_convert_fusion = bf16[1024,1408]{1,0:T(8,128)(2,1)S(1)} fusion(bf16[1024,2048]{1,0:T(8,128)(2,1)} %copy-done.10, bf16[2048,1408]{1,0:T(8,128)(2,1)} %all-gather.6.cloned.1.call-done), kind=kOutput, calls=%fused_computation.12 | convolution fusion | flops 5907021824 | bytes 12845056 | tf_op jit(solution)/shard_map/dot_general | solution.py:532
  217.8 2.5 collective-permute-start.1
  220.2 3.1 maximum_convert_fusion
  223.3 3.1 maximum_convert_fusion.1
  226.4 73.9 %all-gather.8.cloned.1.call-done = bf16[2048,1408]{1,0:T(8,128)(2,1)} async-done(((bf16[256,1408]{1,0:T(8,128)(2,1)}), bf16[2048,1408]{1,0:T(8,128)(2,1)}) %all-gather.8.cloned.1.call-update) | async-done | bytes 5767184 | tf_op jit(solution)/shard_map/all_gather | solution.py:515
  300.3 22.6 %convolution_convert_fusion.2.partial = bf16[1024,2048]{1,0:T(8,128)(2,1)} fusion(bf16[2048,1408]{1,0:T(8,128)(2,1)} %all-gather.8.cloned.1.call-done, f32[1026,1408]{1,0:T(8,128)} %maximum_convert_fusion.1, f32[1026,1408]{1,0:T(8,128)} %maximum_convert_fusion, f32[1408]{0:T(1024)S(1)} %get-tuple-element.16, f32[1408]{0:T(1024)S(1)} %get-tuple-element.17, ...), kind=kOutput, calls=%fused_computation.14 | convolution fusion | flops 5930745856 | bytes 44598272 | tf_op jit(solution)/shard_map/dot_general | solution.py:540
  322.9 2.2 copy-done
  325.1 27.3 %closed.1 = bf16[256,2048]{1,0:T(8,128)(2,1)S(1)} custom-call(bf16[1024,2048]{1,0:T(8,128)(2,1)S(1)} %copy-done, bf16[256,2048]{1,0:T(8,128)(2,1)S(1)} %get-tuple-element.14.stream), custom_call_target="tpu_custom_call" | custom-call | tf_op jit(solution)/shard_map/closed/pallas_call | solution.py:415
  (44 shorter events, 7.0 us)
Async XLA Ops:
  6.5 146.6 %all-gather.4.cloned.1.call-start = ((), (), s32[]{:S(2)}) async-start(), calls=%async_computation | async-start | bytes 6488064 | tf_op jit(solution)/shard_map/all_gather | solution.py:513
  7.3 200.2 %all-gather.6.cloned.1.call-start = ((), (), s32[]{:S(2)}) async-start(), calls=%async_computation.1 | async-start | bytes 6488064 | tf_op jit(solution)/shard_map/all_gather | solution.py:514
  8.0 292.3 %all-gather.8.cloned.1.call-start = ((), (), s32[]{:S(2)}) async-start(), calls=%async_computation.2 | async-start | bytes 6488064 | tf_op jit(solution)/shard_map/all_gather | solution.py:515
  8.7 1.2 copy-start.11
  10.0 1.0 copy-start.12
  11.0 1.0 copy-start.13
  12.1 1.0 copy-start.14
  13.1 1.0 copy-start.15
  14.1 1.0 copy-start.16
  15.2 76.0 %copy-start.19 = (bf16[3,2,1408]{2,1,0:T(2,128)(2,1)S(1)}, bf16[3,2,1408]{2,1,0:T(2,128)(2,1)}, u32[]{:S(2)}) copy-start(bf16[3,2,1408]{2,1,0:T(2,128)(2,1)} %param.29) | copy-start | bytes 50692
  15.2 76.0 %copy-start.2 = (bf16[256,2048]{1,0:T(8,128)(2,1)S(1)}, bf16[256,2048]{1,0:T(8,128)(2,1)}, u32[]{:S(2)}) copy-start(bf16[256,2048]{1,0:T(8,128)(2,1)} %weight_ref.1) | copy-start | bytes 3145732
  15.2 76.0 %copy-start.9 = (f32[256]{0:T(256)S(1)}, f32[256]{0:T(256)}, u32[]{:S(2)}) copy-start(f32[256]{0:T(256)} %param.23) | copy-start | bytes 3076
  15.2 84.8 %copy-start.3 = (bf16[256,2048]{1,0:T(8,128)(2,1)S(1)}, bf16[256,2048]{1,0:T(8,128)(2,1)}, u32[]{:S(2)}) copy-start(bf16[256,2048]{1,0:T(8,128)(2,1)} %residual.1) | copy-start | bytes 3145732
  64.1 1.0 copy-start.4
  65.7 34.3 %copy-start.8 = (f32[2048]{0:T(1024)S(1)}, f32[2048]{0:T(1024)}, u32[]{:S(2)}) copy-start(f32[2048]{0:T(1024)} %param.25) | copy-start | bytes 24580
  91.2 1.0 copy-start.1
  92.3 1.3 copy-start.5
  93.5 1.0 copy-start.6
  151.0 2.0 copy-start.10
  163.9 1.6 copy-start.17
  165.6 54.7 %collective-permute-start = (bf16[2,1408]{1,0:T(2,128)(2,1)S(1)}, bf16[2,1408]{1,0:T(2,128)(2,1)S(1)}, u32[]{:S(2)}, u32[]{:S(2)}) collective-permute-start(bf16[2,1408]{1,0:T(2,128)(2,1)S(1)} %slice.71), channel_id=1, source_target_pairs={{0,4},{4,8},{8,12},{12,16},{16,20},{20,24},{24,28},{1,5},{5,9},{9,... | collective-permute-start | bytes 16904 | tf_op jit(solution)/shard_map/ppermute | solution.py:488
  207.5 12.8 %copy-start.18 = (bf16[1024,1408]{1,0:T(8,128)(2,1)S(1)}, bf16[1024,1408]{1,0:T(8,128)(2,1)}, u32[]{:S(2)}) copy-start(bf16[1024,1408]{1,0:T(8,128)(2,1)} %copy-done.17) | copy-start | bytes 8650756
  217.8 5.6 %collective-permute-start.1 = (bf16[2,1408]{1,0:T(2,128)(2,1)S(1)}, bf16[2,1408]{1,0:T(2,128)(2,1)S(1)}, u32[]{:S(2)}, u32[]{:S(2)}) collective-permute-start(bf16[2,1408]{1,0:T(2,128)(2,1)S(1)} %slice.78), channel_id=1, source_target_pairs={{0,4},{4,8},{8,12},{12,16},{16,20},{20,24},{24,28},{1,5},{5,9},{9,... | collective-permute-start | bytes 16904 | tf_op jit(solution)/shard_map/ppermute | solution.py:488
  322.9 2.2 copy-start
  (1 other events, 0.6 us)
Sparse Core Ops, SparseCore 0:
  9.5 104.1 all-gather.3
  115.9 91.4 all-gather.5
  209.6 90.5 all-gather.7

commit v2 on v1

--- a/solution.py
+++ b/solution.py
@@ -248,7 +248,7 @@
     return half, device, window, step
 
 
-def greet(axis):
+def greet(axis, more=0):
     count = lax.axis_size(axis)
     me = lax.axis_index(axis)
     barrier = pltpu.get_barrier_semaphore()
@@ -256,7 +256,7 @@
         pl.semaphore_signal(
             barrier, inc=1, device_id={axis: lax.rem(me + step, count)}, device_id_type=MESH
         )
-    pl.semaphore_wait(barrier, count - 1)
+    pl.semaphore_wait(barrier, count - 1 + more)
 
 
 def send(axis, source, target, sems, index, device):
@@ -272,7 +272,7 @@
     return copy
 
 
-def summed_pieces(axis, partial, near, leaving, far, near_sems, far_sems, finish):
+def summed_pieces(axis, partial, near, leaving, far, near_sems, far_sems, finish, between=None):
     rows = near.shape[1]
     half, device, window, step = pieces_of(axis, rows)
     order = list(range(1, half)) + [0]
@@ -302,6 +302,8 @@
                 (offset - 1) * PIECES + piece,
                 device(offset, False),
             )
+    if between is not None:
+        between()
     for piece in range(PIECES):
         at = pl.ds(piece * step, step)
         near_copies[0, piece].wait_recv()
@@ -314,12 +316,66 @@
         copy.wait_send()
 
 
+class Ring:
+    def __init__(self, axis, shard, gathered, sems, local_sem):
+        self.axis, self.shard, self.gathered, self.sems = axis, shard, gathered, sems
+        self.count = lax.axis_size(axis)
+        me = lax.axis_index(axis)
+        odd = lax.rem(me, 2)
+        self.place = (1 - odd) * (me // 2) + odd * (self.count - 1 - me // 2)
+        self.ahead = self.count // 2
+        self.behind = self.count - 1 - self.ahead
+        self.hop = 0
+        self.going = {}
+        self.sent = []
+        self.own = pltpu.make_async_copy(shard, self.block(0), local_sem)
+
+    def index(self, offset):
+        at = lax.rem(self.place + offset + 2 * self.count, self.count)
+        upper = at // (self.count // 2)
+        return (1 - upper) * 2 * at + upper * (2 * (self.count - 1 - at) + 1)
+
+    def block(self, offset):
+        rows = self.shard.shape[0]
+        return self.gathered.at[pl.ds(pl.multiple_of(self.index(offset) * rows, rows), rows)]
+
+    def move(self):
+        for copy in self.going.values():
+            copy.wait_recv()
+            self.sent.append(copy)
+        self.going = {}
+        for way, limit, base in ((1, self.ahead, 0), (-1, self.behind, self.ahead)):
+            if self.hop < limit:
+                source = self.shard if self.hop == 0 else self.block(-way * self.hop)
+                self.going[way] = send(
+                    self.axis, source, self.block(-way * self.hop), self.sems,
+                    base + self.hop, self.index(way),
+                )
+        self.hop += 1
+
+    def finish(self):
+        while self.going:
+            self.move()
+        for copy in self.sent:
+            copy.wait_send()
+        self.own.wait()
+
+
 def stream_kernel(
-    axis, partial, residual, gain, stream, whole, near, leaving, far,
+    axis, ring_axis, partial, residual, gain, shard, stream, whole, gathered,
+    near, leaving, far,
     near_send, near_recv, far_send, far_recv, side_send, side_recv, out_send, out_recv,
-    pass_send, pass_recv,
+    pass_send, pass_recv, ring_send, ring_recv, own_sem,
 ):
-    greet(axis)
+    ring = Ring(ring_axis, shard, gathered, (ring_send, ring_recv), own_sem)
+    barrier = pltpu.get_barrier_semaphore()
+    for way in (1, -1):
+        pl.semaphore_signal(
+            barrier, inc=1, device_id={ring_axis: ring.index(way)}, device_id_type=MESH
+        )
+    greet(axis, 2)
+    ring.own.start()
+    ring.move()
     half, device, window, _ = pieces_of(axis, residual.shape[0])
     side_copies = {}
     out_copies = {}
@@ -342,8 +398,10 @@
         )
 
     summed_pieces(
-        axis, partial, near, leaving, far, (near_send, near_recv), (far_send, far_recv), finish
-    )
+        axis, partial, near, leaving, far, (near_send, near_recv), (far_send, far_recv), finish,
+        ring.move,
+    )
+    ring.move()
     for piece in range(PIECES):
         for offset in range(1, half):
             out_copies[offset, piece].wait_recv()
@@ -352,6 +410,7 @@
                 axis, whole.at[arrived], whole.at[arrived], (pass_send, pass_recv),
                 (offset - 1) * PIECES + piece, device(0, True),
             )
+    ring.finish()
     for copy in list(out_copies.values()):
         copy.wait_send()
     for copy in list(side_copies.values()) + list(pass_copies.values()):
@@ -386,27 +445,31 @@
     ]
 
 
-def streamed(partial, residual, gain, axis, identity):
+def streamed(partial, residual, gain, shard, axis, ring, identity):
+    around = lax.axis_size(ring)
+    hops = around - 1
     rows, features = residual.shape
     dma = pltpu.SemaphoreType.DMA
     others = (lax.axis_size(axis) // 2 - 1) * PIECES
     in_vmem = pl.BlockSpec(memory_space=pltpu.VMEM)
     return pl.pallas_call(
-        functools.partial(stream_kernel, axis),
-        in_specs=[in_vmem] * 3,
-        out_specs=[in_vmem] * 2,
+        functools.partial(stream_kernel, axis, ring),
+        in_specs=[in_vmem] * 4,
+        out_specs=[in_vmem] * 2 + [pl.BlockSpec(memory_space=pl.ANY)],
         out_shape=[
             jax.ShapeDtypeStruct((rows, features), NARROW),
             jax.ShapeDtypeStruct(partial.shape, NARROW),
+            jax.ShapeDtypeStruct((around * shard.shape[0], shard.shape[1]), NARROW),
         ],
         scratch_shapes=sum_scratch(axis, rows, features)
         + [dma((PIECES,)), dma((PIECES,))]
-        + [dma((others,))] * 4,
+        + [dma((others,))] * 4
+        + [dma((hops,)), dma((hops,)), dma],
         compiler_params=pltpu.CompilerParams(
             collective_id=identity, has_side_effects=True, vmem_limit_bytes=40 * 1024 * 1024
         ),
         name="streamed",
-    )(partial, residual, gain[None])
+    )(partial, residual, gain[None], shard)
 
 
 def closed(partial, stream, axis, identity):
@@ -512,7 +575,6 @@
 ):
     full_gate = lax.all_gather(gate_projection_weight, "sp", axis=0, tiled=True)
     full_up = lax.all_gather(up_projection_weight, "sp", axis=0, tiled=True)
-    full_down = lax.all_gather(down_projection_weight, "sp", axis=0, tiled=True)
     local, reach, own_map = recurrence(
         receptance,
         key_matrix_all,
@@ -525,8 +587,14 @@
     partial = project(
         local, reach, maps, head_norm_gain, output_gate_all_heads, output_projection_weight
     )
-    stream, whole_rows = streamed(
-        partial, residual_input_stream, feedforward_norm_gain, "tp", 2
+    stream, whole_rows, full_down = streamed(
+        partial,
+        residual_input_stream,
+        feedforward_norm_gain,
+        down_projection_weight,
+        "tp",
+        "sp",
+        2,
     )
     gate_acc = jnp.dot(whole_rows, full_gate, preferred_element_type=jnp.float32)
     up_acc = jnp.dot(whole_rows, full_up, preferred_element_type=jnp.float32)

time: 360 us -> 344 us (0.956)
  waiting for transfers between devices: 116 us -> 1.45 us
  Pallas kernels: 158 us -> 243 us
  starting transfers between devices: 4.49 us -> 19.5 us
    pallas_call x1, Pallas kernels: 51 us -> 136 us  [streamed(): pl.pallas_call(functools.partial(stream_kernel, axis, ring), in_specs=[in...]
    all_gather x1 -> x0, waiting for transfers between devices: 73.9 us -> none  [body(): full_down = lax.all_gather(down_projection_weight, 'sp', axis=0, tiled=True)]
    all_gather x1, waiting for transfers between devices: 39.9 us -> 0.02 us  [body(): full_up = lax.all_gather(up_projection_weight, 'sp', axis=0, tiled=True)]
    ppermute x2, starting transfers between devices: 4.41 us -> 19.5 us  [passed_along(): return lax.ppermute(x, axis, pairs)]
    unnamed x41 -> x39, local copies, waits for them, and re-layouts: 18.1 us -> 15.9 us
  transfers between devices with their start and end apart: 5 -> 4, of which waited for: 2 -> 0; matrix products, arithmetic and copies ran while one was open for 8% -> 7% of each run, Pallas kernels for 36% -> 63%
where the time goes in v2:
time: 344 us; the launch traced here: 343 us
  Pallas kernels  243 us (71%)
  matrix products  42.9 us (12%)
  starting transfers between devices  19.5 us (6%)
  local copies, waits for them, and re-layouts  16 us (5%)
  between operations  13.6 us (4%)
  other arithmetic  6.2 us (2%)
    pallas_call x1, Pallas kernels, streamed(): pl.pallas_call(functools.partial(stream_kernel, axis, ring), in_specs=[in...  136 us
    pallas_call x1, Pallas kernels, recurrence(): pl.pallas_call(recurrence_kernel, grid=(tokens // rows,), in_specs=[spec]...  48.9 us
    pallas_call x1, Pallas kernels, closed(): pl.pallas_call(functools.partial(closing_kernel, axis), in_specs=[in_vmem...  27.3 us
    pallas_call x1, Pallas kernels, exchange(): pl.pallas_call(functools.partial(exchange_kernel, axis), out_shape=jax.Sh...  25.5 us
    dot_general x1, matrix products, body(): lax.dot_general(hidden, full_down, (((1,), (1,)), ((), ())), preferred_el...  22.5 us
    ppermute x2, starting transfers between devices, passed_along(): return lax.ppermute(x, axis, pairs)  19.5 us
    unnamed x39, local copies, waits for them, and re-layouts  15.9 us
    dot_general x1, matrix products, body(): up_acc = jnp.dot(whole_rows, full_up, preferred_element_type=jnp.float32)  10.3 us
  transfers between devices with their start and end apart: 4, of which 0 were waited for; matrix products, arithmetic and copies ran while one was open for 7% of the time, Pallas kernels for 63%

profile of v2, /device:TPU:0, one launch (start us, length us, event | category | flops | bytes accessed | tf_op | source)
XLA Modules:
  0.0 342.7 jit_solution(16443904238013528318)
XLA Ops:
  8.0 1.2 copy-done.10
  9.2 1.0 copy-done.11
  10.3 1.0 copy-done.12
  11.3 1.0 copy-done.13
  12.4 1.0 copy-done.14
  13.4 1.0 copy-done.15
  14.4 48.9 %recurrence.1 = (f32[1024,256]{1,0:T(8,128)S(1)}, f32[1024,256]{1,0:T(8,128)S(1)}, bf16[64,512]{1,0:T(8,128)(2,1)S(1)}) custom-call(bf16[1024,256]{1,0:T(8,128)(2,1)S(1)} %copy-done.11, bf16[1024,256]{1,0:T(8,128)(2,1)S(1)} %copy-done.12, bf16[1024,256]{1,0:T(8,128)(2,1)S(1)} %copy-done.13, bf16[1024,256]{1,0:T(8,128)(2,1)S(1)} %copy-done.14, ...), custom_call_target="tpu_custom_call" | custom-call | flops 33554432000 | bytes 4194304 | tf_op jit(solution)/shard_map/recurrence/pallas_call | solution.py:166
  64.0 25.5 %exchange.1.maps_ref = bf16[8,64,512]{2,1,0:T(8,128)(2,1)} custom-call(bf16[64,512]{1,0:T(8,128)(2,1)} %copy-done.6), custom_call_target="tpu_custom_call" | custom-call | tf_op jit(solution)/shard_map/exchange/pallas_call | solution.py:218
  89.5 1.0 copy-done.1
  90.5 1.0 copy-done.5
  91.6 5.4 %project.1.partial = bf16[1024,2048]{1,0:T(8,128)(2,1)S(1)} custom-call(f32[1024,256]{1,0:T(8,128)S(1)} %get-tuple-element.11.local_ref, f32[1024,256]{1,0:T(8,128)S(1)} %get-tuple-element.12.reach_ref, bf16[8,64,512]{2,1,0:T(8,128)(2,1)S(1)} %copy-done.1, f32[1,256]{1,0:T(1,128)S(1)} %bitcast.8, bf16[1024,256]{1,0:T(8,128)(2,1)S(1)} %copy-done.5, ...), custom_call_target="tpu_custom_call" | custom-call | tf_op jit(solution)/shard_map/project/pallas_call | solution.py:527
  97.0 136.1 %streamed.1 = (bf16[256,2048]{1,0:T(8,128)(2,1)S(1)}, bf16[1024,2048]{1,0:T(8,128)(2,1)S(1)}, bf16[2048,1408]{1,0:T(8,128)(2,1)}) custom-call(bf16[1024,2048]{1,0:T(8,128)(2,1)S(1)} %project.1.partial, bf16[256,2048]{1,0:T(8,128)(2,1)S(1)} %copy-done.3, f32[1,2048]{1,0:T(1,128)S(1)} %bitcast.7, bf16[256,1408]{1,0:T(8,128)(2,1)S(1)} %copy-done.4), custom_call_target="tpu_custom_call" | custom-call | tf_op jit(solution)/shard_map/streamed/pallas_call | solution.py:455
  233.1 1.9 copy-done.9
  235.2 10.1 %convolution_convert_fusion.1 = bf16[1024,1408]{1,0:T(8,128)(2,1)S(1)} fusion(bf16[1024,2048]{1,0:T(8,128)(2,1)} %copy-done.9, bf16[2048,1408]{1,0:T(8,128)(2,1)} %all-gather.3.cloned.1.call-done), kind=kOutput, calls=%fused_computation.13 | convolution fusion | flops 5907021824 | bytes 12845056 | tf_op jit(solution)/shard_map/dot_general | solution.py:599
  245.3 1.6 copy-done.16
  247.0 17.5 %collective-permute-start = (bf16[2,1408]{1,0:T(2,128)(2,1)S(1)}, bf16[2,1408]{1,0:T(2,128)(2,1)S(1)}, u32[]{:S(2)}, u32[]{:S(2)}) collective-permute-start(bf16[2,1408]{1,0:T(2,128)(2,1)S(1)} %slice.71), channel_id=1, source_target_pairs={{0,4},{4,8},{8,12},{12,16},{16,20},{20,24},{24,28},{1,5},{5,9},{9,... | collective-permute-start | bytes 16904 | tf_op jit(solution)/shard_map/ppermute | solution.py:551
  264.6 10.3 %convolution_convert_fusion = bf16[1024,1408]{1,0:T(8,128)(2,1)S(1)} fusion(bf16[1024,2048]{1,0:T(8,128)(2,1)} %copy-done.9, bf16[2048,1408]{1,0:T(8,128)(2,1)} %all-gather.5.cloned.1.call-done), kind=kOutput, calls=%fused_computation.12 | convolution fusion | flops 5907021824 | bytes 12845056 | tf_op jit(solution)/shard_map/dot_general | solution.py:600
  274.9 1.9 collective-permute-start.1
  276.8 3.1 maximum_convert_fusion
  279.9 3.1 maximum_convert_fusion.1
  283.0 22.5 %convolution_convert_fusion.2.partial = bf16[1024,2048]{1,0:T(8,128)(2,1)} fusion(bf16[2048,1408]{1,0:T(8,128)(2,1)} %get-tuple-element.15, f32[1026,1408]{1,0:T(8,128)} %maximum_convert_fusion.1, f32[1026,1408]{1,0:T(8,128)} %maximum_convert_fusion, f32[1408]{0:T(1024)S(1)} %get-tuple-element.18, f32[1408]{0:T(1024)S(1)} %get-tuple-element.19, ...), kind=kOutput, calls=%fused_computation.14 | convolution fusion | flops 5930745856 | bytes 44598272 | tf_op jit(solution)/shard_map/dot_general | solution.py:608
  305.5 2.2 copy-done
  307.7 27.3 %closed.1 = bf16[256,2048]{1,0:T(8,128)(2,1)S(1)} custom-call(bf16[1024,2048]{1,0:T(8,128)(2,1)S(1)} %copy-done, bf16[256,2048]{1,0:T(8,128)(2,1)S(1)} %get-tuple-element.16.stream), custom_call_target="tpu_custom_call" | custom-call | tf_op jit(solution)/shard_map/closed/pallas_call | solution.py:478
  334.9 1.0 copy.17
  (39 shorter events, 2.3 us)
Async XLA Ops:
  6.5 228.7 %all-gather.3.cloned.1.call-start = ((), (), s32[]{:S(2)}) async-start(), calls=%async_computation | async-start | bytes 6488064 | tf_op jit(solution)/shard_map/all_gather | solution.py:576
  7.3 257.3 %all-gather.5.cloned.1.call-start = ((), (), s32[]{:S(2)}) async-start(), calls=%async_computation.1 | async-start | bytes 6488064 | tf_op jit(solution)/shard_map/all_gather | solution.py:577
  8.0 1.2 copy-start.10
  9.2 1.0 copy-start.11
  10.3 1.0 copy-start.12
  11.3 1.0 copy-start.13
  12.4 1.0 copy-start.14
  13.4 1.0 copy-start.15
  14.4 75.0 %copy-start.18 = (bf16[3,2,1408]{2,1,0:T(2,128)(2,1)S(1)}, bf16[3,2,1408]{2,1,0:T(2,128)(2,1)}, u32[]{:S(2)}) copy-start(bf16[3,2,1408]{2,1,0:T(2,128)(2,1)} %param.29) | copy-start | bytes 50692
  14.4 75.0 %copy-start.2 = (bf16[256,2048]{1,0:T(8,128)(2,1)S(1)}, bf16[256,2048]{1,0:T(8,128)(2,1)}, u32[]{:S(2)}) copy-start(bf16[256,2048]{1,0:T(8,128)(2,1)} %weight_ref.1) | copy-start | bytes 3145732
  14.4 75.0 %copy-start.8 = (f32[256]{0:T(256)S(1)}, f32[256]{0:T(256)}, u32[]{:S(2)}) copy-start(f32[256]{0:T(256)} %param.23) | copy-start | bytes 3076
  63.3 0.6 copy-start.6
  64.0 33.0 %copy-start.7 = (f32[2048]{0:T(1024)S(1)}, f32[2048]{0:T(1024)}, u32[]{:S(2)}) copy-start(f32[2048]{0:T(1024)} %param.25) | copy-start | bytes 24580
  89.5 1.0 copy-start.1
  90.5 1.0 copy-start.5
  91.6 5.4 %copy-start.3 = (bf16[256,2048]{1,0:T(8,128)(2,1)S(1)}, bf16[256,2048]{1,0:T(8,128)(2,1)}, u32[]{:S(2)}) copy-start(bf16[256,2048]{1,0:T(8,128)(2,1)} %residual.1) | copy-start | bytes 3145732
  91.6 5.4 %copy-start.4 = (bf16[256,1408]{1,0:T(8,128)(2,1)S(1)}, bf16[256,1408]{1,0:T(8,128)(2,1)}, u32[]{:S(2)}) copy-start(bf16[256,1408]{1,0:T(8,128)(2,1)} %shard.1) | copy-start | bytes 2162692
  233.1 2.0 copy-start.9
  245.3 1.6 copy-start.16
  247.0 29.8 %collective-permute-start = (bf16[2,1408]{1,0:T(2,128)(2,1)S(1)}, bf16[2,1408]{1,0:T(2,128)(2,1)S(1)}, u32[]{:S(2)}, u32[]{:S(2)}) collective-permute-start(bf16[2,1408]{1,0:T(2,128)(2,1)S(1)} %slice.71), channel_id=1, source_target_pairs={{0,4},{4,8},{8,12},{12,16},{16,20},{20,24},{24,28},{1,5},{5,9},{9,... | collective-permute-start | bytes 16904 | tf_op jit(solution)/shard_map/ppermute | solution.py:551
  264.6 12.2 %copy-start.17 = (bf16[1024,1408]{1,0:T(8,128)(2,1)S(1)}, bf16[1024,1408]{1,0:T(8,128)(2,1)}, u32[]{:S(2)}) copy-start(bf16[1024,1408]{1,0:T(8,128)(2,1)} %copy-done.16) | copy-start | bytes 8650756
  274.9 5.1 %collective-permute-start.1 = (bf16[2,1408]{1,0:T(2,128)(2,1)S(1)}, bf16[2,1408]{1,0:T(2,128)(2,1)S(1)}, u32[]{:S(2)}, u32[]{:S(2)}) collective-permute-start(bf16[2,1408]{1,0:T(2,128)(2,1)S(1)} %slice.78), channel_id=1, source_target_pairs={{0,4},{4,8},{8,12},{12,16},{16,20},{20,24},{24,28},{1,5},{5,9},{9,... | collective-permute-start | bytes 16904 | tf_op jit(solution)/shard_map/ppermute | solution.py:551
  305.5 2.2 copy-start
Sparse Core Ops, SparseCore 0:
  9.5 107.8 all-gather.2
  119.6 127.1 all-gather.4
